TPU v7x, 128 devices: a whole 4x4x4 slice. The times are simulated.
128 devices in a mesh: ep: 64 (over z, y, x), tp: 2 (over core).
Axes of the slice: x: 4, y: 4, z: 4, core: 2. Of those that a mesh axis runs over, the one named last changes fastest.
Arguments:
- tokens: bfloat16 [32768, 2048], P(('ep', 'tp')), may hold values from -6 to 6
- norm_gain: float32 [2048], replicated, may hold values from 0.1 to 1.9
- norm_bias: float32 [2048], replicated, may hold values from -3 to 3
- gate_weight: bfloat16 [64, 2048, 1024], P('ep', None, 'tp'), may hold values from -0.125 to 0.125
- up_weight: bfloat16 [64, 2048, 1024], P('ep', None, 'tp'), may hold values from -0.125 to 0.125
- down_weight: bfloat16 [64, 1024, 2048], P('ep', 'tp'), may hold values from -0.1875 to 0.1875
- expert_ids: int32 [32768, 2], P(('ep', 'tp')), may hold values from 0 to 63, all different within a row; in each aligned block of 256 rows (0 to 255, 256 to 511, ...) at most 16 rows name the same one
- route_weights: float32 [32768, 2], P(('ep', 'tp')), may hold values from 0.2 to 1
Outputs:
- mixed: bfloat16 [32768, 2048], P(('ep', 'tp'))
Inputs may be any that keep to these rules, and one draw needn't show every extreme that they name: `expert_ids`: a token's 2 experts differ; in the tokens of one device (aligned blocks of 256 rows) no expert is named by more than 16 entries, a bound that some block reaches.
All inputs are finite; a program needn't handle non-finite values.
Results may differ from a plain program's by a relative error of at most 0.0071.
Values may be sent and summed in bfloat16 or wider, within the bound.
A program may use at most 128 MiB of HBM per device.

v0:
```python
import functools

import jax
import jax.numpy as jnp
from jax import lax
from jax.experimental import pallas as pl
from jax.experimental.pallas import tpu as pltpu
from jax.sharding import PartitionSpec as P

MESH = pl.DeviceIdType.MESH
LINE = 4
CHUNKS = 8
LAG = 2


def kernel(
    planes, raw, gain, bias, meta, gw, uw, dw, out,
    src, tok, met, wg, wu, wd, sel, mix, snd, xin, hid, res, ret, psend, racc,
    s_own, s_met, s_mets, s_wl, s_ws, s_wr, s_tok, s_toks, s_x, s_xs, s_r, s_rs, s_p, s_ps,
):
    n = LINE
    side = planes
    me, core = lax.axis_index("ep"), lax.axis_index("tp")
    z, p = me // side, lax.rem(me, side)
    tokens, width = raw.shape
    half = gw.shape[2]
    rows = snd.shape[1]
    cap = rows // side
    k = CHUNKS
    wide = width // k
    end = (z == 0) | (z == n - 1)
    mid = jnp.logical_not(end)
    step = jnp.where(z < n // 2, 1, -1)
    za, zb = z + step, z - step
    order = [
        z,
        jnp.where(end, z + 3 * step, z + 2 * step),
        jnp.where(end, z + 2 * step, z - step),
        z + step,
    ]

    def cols(c):
        return pl.ds(pl.multiple_of(c * wide, wide), wide)

    def band(i):
        return pl.ds(pl.multiple_of(i * cap, cap), cap)

    def plane(t):
        return {"ep": t * side + p}

    def peer(j):
        return lax.rem(p + j, side)

    def remote(src, dst, send, recv, where):
        return pltpu.make_async_remote_copy(
            src_ref=src, dst_ref=dst, send_sem=send, recv_sem=recv,
            device_id=where, device_id_type=MESH,
        )

    def landed(ref, sem):
        pltpu.make_async_copy(ref, ref, sem).wait()

    barrier = pltpu.get_barrier_semaphore()
    own = pltpu.make_async_copy(raw, src, s_own.at[0])
    own.start()
    ownm = pltpu.make_async_copy(meta, met.at[z], s_own.at[1])
    ownm.start()
    for j in range(1, side):
        pl.semaphore_signal(
            barrier, inc=1, device_id={"ep": z * side + peer(j)}, device_id_type=MESH
        )
    for j in range(1, n):
        pl.semaphore_signal(
            barrier, inc=1, device_id=plane(lax.rem(z + j, n)), device_id_type=MESH
        )
    pl.semaphore_signal(barrier, inc=1, device_id={"tp": 1 - core}, device_id_type=MESH)

    def send_tok(s, c, to, way):
        remote(
            tok.at[s, :, cols(c)], tok.at[s, :, cols(c)],
            s_toks.at[way, s], s_tok.at[s, c], plane(to),
        ).start()

    def send_own(to, way):
        @pl.loop(0, k)
        def _(c):
            send_tok(z, c, to, way)

    def prep(q):
        s = order[q]
        ids0, ids1 = met[s, 0:1, :], met[s, 1:2, :]
        wt0, wt1 = met[s, 2:3, :], met[s, 3:4, :]
        row = lax.broadcasted_iota(jnp.int32, (rows, tokens), 0)
        e_row = (z * side + row // cap).astype(jnp.float32)
        s_row = lax.rem(row, cap).astype(jnp.float32)
        hit0 = (ids0 == e_row).astype(jnp.float32)
        hit1 = (ids1 == e_row).astype(jnp.float32)
        hit = hit0 + hit1
        before = (
            lax.broadcasted_iota(jnp.int32, (tokens, tokens), 0)
            < lax.broadcasted_iota(jnp.int32, (tokens, tokens), 1)
        ).astype(jnp.float32).astype(jnp.bfloat16)
        count = jnp.dot(hit.astype(jnp.bfloat16), before, preferred_element_type=jnp.float32)
        pick = jnp.where(count == s_row, hit, 0.0)
        sel[q] = pick.astype(jnp.bfloat16)
        w = pick * (hit0 * wt0 + hit1 * wt1)
        high = w.astype(jnp.bfloat16)
        mix[q, 0] = high
        mix[q, 1] = (w - high.astype(jnp.float32)).astype(jnp.bfloat16)

    own.wait()
    slab = min(32, tokens)

    @pl.loop(0, tokens // slab)
    def _(i):
        at = pl.ds(pl.multiple_of(i * slab, slab), slab)
        v = src[at, :].astype(jnp.float32)
        v = v - jnp.mean(v, axis=-1, keepdims=True)
        spread = jnp.mean(v * v, axis=-1, keepdims=True)
        y = v * lax.rsqrt(spread + 1e-05) * gain[...] + bias[...]
        tok[z, at, :] = y.astype(jnp.bfloat16)

    ownm.wait()
    prep(0)
    pl.semaphore_wait(barrier, side - 1 + n)
    for j in range(1, n):
        remote(
            met.at[z], met.at[z], s_mets.at[j - 1], s_met.at[z], plane(lax.rem(z + j, n))
        ).start()

    @pl.when(end)
    def _():
        send_own(za, 0)

    halfrows = pl.ds(pl.multiple_of(core * half, half), half)
    pairs = [
        (gw.at[0], wg.at[core]), (uw.at[0], wu.at[core]), (dw.at[0], wd.at[halfrows]),
    ]
    for i, (a, b) in enumerate(pairs):
        pltpu.make_async_copy(a, b, s_wl.at[i]).start()
        remote(a, b, s_ws.at[i], s_wr.at[i], {"tp": 1 - core}).start()

    def disp(q, c):
        y = jnp.dot(sel[q], tok[order[q], :, cols(c)], preferred_element_type=jnp.float32)
        snd[q, :, cols(c)] = y.astype(jnp.bfloat16)
        xin[q, band(p), cols(c)] = snd[q, band(p), cols(c)]
        for j in range(1, side):
            o = peer(j)
            remote(
                snd.at[q, band(o), cols(c)], xin.at[q, band(p), cols(c)],
                s_xs.at[q], s_x.at[q], {"ep": z * side + o},
            ).start()

    def others(ref, q):
        return ref.at[q, pl.ds(0, (side - 1) * cap)]

    tile = min(256, half)
    per = half // tile

    def gate(q, i):
        h, at = i // per, lax.rem(i, per)
        part = pl.ds(pl.multiple_of(at * tile, tile), tile)
        x = xin[q]
        g = jnp.dot(x, wg[h, :, part], preferred_element_type=jnp.float32)
        u = jnp.dot(x, wu[h, :, part], preferred_element_type=jnp.float32)
        v = g / (1.0 + jnp.exp(-g)) * u
        hid[:, pl.ds(pl.multiple_of(i * tile, tile), tile)] = v.astype(jnp.bfloat16)

    def down(q):
        @pl.loop(0, k)
        def _(c):
            y = jnp.dot(hid[...], wd[:, cols(c)], preferred_element_type=jnp.float32)
            res[q, :, cols(c)] = y.astype(jnp.bfloat16)
            ret[q, band(p), cols(c)] = res[q, band(p), cols(c)]
            for j in range(1, side):
                o = peer(j)
                remote(
                    res.at[q, band(o), cols(c)], ret.at[q, band(p), cols(c)],
                    s_rs.at[q], s_r.at[q, c], {"ep": z * side + o},
                ).start()

    def compute(q):
        landed(others(xin, q), s_x.at[q])
        pl.loop(0, 2 * per)(lambda i: gate(q, i))
        down(q)

    def weigh(q, c):
        landed(ret.at[q, pl.ds(0, (side - 1) * cap), cols(c)], s_r.at[q, c])
        r = ret[q, :, cols(c)]
        dims = (((0,), (0,)), ((), ()))
        return lax.dot_general(
            mix[q, 0], r, dims, preferred_element_type=jnp.float32
        ) + lax.dot_general(mix[q, 1], r, dims, preferred_element_type=jnp.float32)

    def combine(q, c, add):
        t = order[q]
        y = weigh(q, c)
        to = zb if (q == 2 and add) else za
        if add:
            landed(racc.at[t, c], s_p.at[t, c])
            y = y + racc[t, c].astype(jnp.float32)
        psend[q - 1, c] = y.astype(jnp.bfloat16)
        slot = jnp.where((to == t) & (to < z), n, t)
        remote(
            psend.at[q - 1, c], racc.at[slot, c], s_ps.at[q - 1], s_p.at[slot, c], plane(to)
        ).start()

    def arrived(s, c):
        landed(tok.at[s, :, cols(c)], s_tok.at[s, c])

    @pl.loop(0, k)
    def _(c):
        disp(0, c)

    for q in range(1, n):
        landed(met.at[order[q]], s_met.at[order[q]])
        prep(q)

    def near(c):
        arrived(order[2], c)
        send_tok(order[2], c, za, 0)
        disp(2, c)

    def far(c):
        arrived(order[1], c)
        send_tok(order[1], c, zb, 1)
        disp(1, c)

    def weights():
        for i, (a, b) in enumerate(pairs):
            pltpu.make_async_copy(a, b, s_wl.at[i]).wait()
            landed(b, s_wr.at[i])

    @pl.when(mid)
    def _():
        def pass_on(c):
            arrived(order[3], c)
            send_tok(order[3], c, zb, 1)
            disp(3, c)

        for c in range(LAG):
            near(c)

        @pl.loop(LAG, k)
        def _(c):
            near(c)
            far(c - LAG)

        send_own(za, 0)
        pl.loop(k - LAG, k)(far)
        weights()
        pl.loop(0, k // 2)(pass_on)
        landed(others(xin, 1), s_x.at[1])
        turns = k - k // 2
        for j in range(turns):
            pass_on(k // 2 + j)
            for i in range(j * 2 * per // turns, (j + 1) * 2 * per // turns):
                gate(1, i)
        send_own(zb, 1)
        down(1)
        compute(2)
        compute(3)
        for c in range(LAG):
            combine(1, c, True)

        @pl.loop(LAG, k)
        def _(c):
            combine(1, c, True)
            combine(2, c - LAG, True)

        pl.loop(k - LAG, k)(lambda c: combine(2, c, True))
        compute(0)
        pl.loop(0, k)(lambda c: combine(3, c, True))

    @pl.when(end)
    def _():
        def take(c):
            arrived(order[1], c)
            disp(1, c)

        pl.loop(0, k // 2)(take)
        weights()
        compute(0)
        pl.loop(k // 2, k)(take)
        compute(1)

        @pl.loop(0, k)
        def _(c):
            arrived(order[2], c)
            disp(2, c)
            combine(1, c, False)

        compute(2)

        @pl.loop(0, k)
        def _(c):
            combine(2, c, False)
            arrived(order[3], c)
            disp(3, c)

        compute(3)
        pl.loop(0, k)(lambda c: combine(3, c, False))

    def last(c, slots):
        y = weigh(0, c)
        for slot in slots:
            landed(racc.at[slot, c], s_p.at[slot, c])
            y = y + racc[slot, c].astype(jnp.float32)
        out[:, cols(c)] = y.astype(out.dtype)

    @pl.when(end)
    def _():
        pl.loop(0, k)(lambda c: last(c, [jnp.where(z == 0, n, z)]))

    @pl.when(mid)
    def _():
        pl.loop(0, k)(lambda c: last(c, [z, n]))

    drain = landed

    for j in range(1, n):
        drain(met.at[z], s_mets.at[j - 1])
    for i, (a, b) in enumerate(pairs):
        drain(b, s_ws.at[i])
    drain(tok.at[z], s_toks.at[0, z])

    @pl.when(mid)
    def _():
        drain(tok.at[z], s_toks.at[1, z])
        drain(tok.at[z], s_toks.at[0, order[2]])
        drain(tok.at[z], s_toks.at[1, order[1]])
        drain(tok.at[z], s_toks.at[1, order[3]])

    for q in range(n):
        drain(others(snd, q), s_xs.at[q])
        drain(others(res, q), s_rs.at[q])
    for q in range(1, n):
        drain(psend.at[q - 1], s_ps.at[q - 1])


def body(
    tokens, norm_gain, norm_bias, gate_weight, up_weight, down_weight, expert_ids, route_weights
):
    count, width = tokens.shape
    experts = lax.axis_size("ep")
    cap = max(4 * count // experts, 4)
    side = experts // LINE
    half = gate_weight.shape[2]
    both = jnp.concatenate([expert_ids.astype(jnp.float32), route_weights], axis=1)
    meta = jnp.pad(both.T, ((0, 4), (0, 0)))
    rows = side * cap
    wide = width // CHUNKS
    bf = jnp.bfloat16
    dma = pltpu.SemaphoreType.DMA
    vmem = pl.BlockSpec(memory_space=pltpu.VMEM)
    hbm = pl.BlockSpec(memory_space=pl.ANY)
    return pl.pallas_call(
        functools.partial(kernel, side),
        out_shape=jax.ShapeDtypeStruct((count, width), bf),
        in_specs=[hbm, vmem, vmem] + [hbm] * 4,
        out_specs=pl.BlockSpec(memory_space=pltpu.VMEM),
        scratch_shapes=[
            pltpu.VMEM((count, width), bf),
            pltpu.VMEM((LINE, count, width), bf),
            pltpu.VMEM((LINE, 8, count), jnp.float32),
            pltpu.VMEM((2, width, half), bf),
            pltpu.VMEM((2, width, half), bf),
            pltpu.VMEM((2 * half, width), bf),
            pltpu.VMEM((LINE, rows, count), bf),
            pltpu.VMEM((LINE, 2, rows, count), bf),
            pltpu.VMEM((LINE, rows, width), bf),
            pltpu.VMEM((LINE, rows, width), bf),
            pltpu.VMEM((rows, 2 * half), bf),
            pltpu.VMEM((LINE, rows, width), bf),
            pltpu.VMEM((LINE, rows, width), bf),
            pltpu.VMEM((LINE - 1, CHUNKS, count, wide), bf),
            pltpu.VMEM((LINE + 1, CHUNKS, count, wide), bf),
            dma((2,)),
            dma((LINE,)),
            dma((LINE - 1,)),
            dma((3,)),
            dma((3,)),
            dma((3,)),
            dma((LINE, CHUNKS)),
            dma((2, LINE)),
            dma((LINE,)),
            dma((LINE,)),
            dma((LINE, CHUNKS)),
            dma((LINE,)),
            dma((LINE + 1, CHUNKS)),
            dma((LINE - 1,)),
        ],
        compiler_params=pltpu.CompilerParams(
            collective_id=0, has_side_effects=True, vmem_limit_bytes=60 * 1024 * 1024
        ),
    )(tokens, norm_gain[None], norm_bias[None], meta, gate_weight, up_weight, down_weight)


def solution(mesh):
    placed = (
        P(("ep", "tp"), None),
        P(),
        P(),
        P("ep", None, "tp"),
        P("ep", None, "tp"),
        P("ep", "tp", None),
        P(("ep", "tp"), None),
        P(("ep", "tp"), None),
    )
    return jax.shard_map(
        body, mesh=mesh, in_specs=placed, out_specs=P(("ep", "tp"), None), check_vma=False
    )
```

profile of v0, /device:TPU:0, one launch (start us, length us, event | category | flops | bytes accessed | tf_op | source)
XLA Modules:
  0.0 139.4 jit_solution(8876791357888166664)
XLA Ops:
  0.0 0.7 convert_element_type.5
  0.7 0.7 maximum_bitcast_fusion
  1.4 0.6 pad.4.meta
  2.0 135.1 %shard_map.82 = bf16[256,2048]{1,0:T(8,128)(2,1)} custom-call(bf16[256,2048]{1,0:T(8,128)(2,1)} %raw.1, f32[1,2048]{1,0:T(1,128)} %bitcast.4, f32[1,2048]{1,0:T(1,128)} %bitcast.5, f32[8,256]{1,0:T(8,128)} %pad.4.meta, bf16[1,2048,512]{2,1,0:T(8,128)(2,1)} %gw.1, bf16[1,2048,512]{2,1,0:T(8,128)(2,1)} %uw.1, bf16[1,512,2048]{2,1,0:T(8,128)(2,1)} %dw.1), custom_call_target="tpu_custom_call" | custom-call | tf_op jit(solution)/shard_map/pallas_call | solution.py:357
  137.0 2.3 %copy.10 = bf16[256,2048]{1,0:T(8,128)(2,1)} copy(bf16[256,2048]{1,0:T(8,128)(2,1)} %shard_map.82) | data formatting | bytes 2097152
where the time goes:
time: 141 us; the launch traced here: 139 us
  Pallas kernels  135 us (96%)
  local copies, waits for them, and re-layouts  2.91 us (2%)
    pallas_call x1, Pallas kernels, body(): pl.pallas_call(functools.partial(kernel, side), out_shape=jax.ShapeDtypeS...  135 us

commit v1 on v0

v1 whole, which is shorter than its diff:
```python
import functools

import jax
import jax.numpy as jnp
from jax import lax
from jax.experimental import pallas as pl
from jax.experimental.pallas import tpu as pltpu
from jax.sharding import PartitionSpec as P

MESH = pl.DeviceIdType.MESH
LINE = 4
CHUNKS = 8
HALF = CHUNKS // 2


def kernel(
    planes, raw, gain, bias, idsin, wtin, gw, uw, dw, out,
    src, gn, bs, ids, wts, tok, met, wg, wu, wd, sel, mix, snd, xin, hid, res, ret, psend, racc,
    fin, s_own, s_met, s_mets, s_wl, s_ws, s_wr, s_tok, s_toks, s_x, s_xs, s_r, s_rs, s_p, s_ps, s_o,
):
    n = LINE
    side = planes
    me, core = lax.axis_index("ep"), lax.axis_index("tp")
    z, p = me // side, lax.rem(me, side)
    tokens, width = raw.shape
    half = gw.shape[2]
    rows = snd.shape[1]
    cap = rows // side
    k = CHUNKS
    wide = width // k

    def cols(c):
        return pl.ds(pl.multiple_of(c * wide, wide), wide)

    def band(i):
        return pl.ds(pl.multiple_of(i * cap, cap), cap)

    def plane(j):
        return {"ep": lax.rem(z + j, n) * side + p}

    up, over, back = 1, 2, n - 1

    def peer(j):
        return lax.rem(p + j, side)

    def remote(src, dst, send, recv, where):
        return pltpu.make_async_remote_copy(
            src_ref=src, dst_ref=dst, send_sem=send, recv_sem=recv,
            device_id=where, device_id_type=MESH,
        )

    def landed(ref, sem):
        pltpu.make_async_copy(ref, ref, sem).wait()

    firsts = [
        pltpu.make_async_copy(a, b, s_own.at[i])
        for i, (a, b) in enumerate(
            [(raw, src), (gain, gn), (bias, bs), (idsin, ids), (wtin, wts)]
        )
    ]
    for copy in firsts:
        copy.start()
    barrier = pltpu.get_barrier_semaphore()
    for j in range(1, side):
        pl.semaphore_signal(
            barrier, inc=1, device_id={"ep": z * side + peer(j)}, device_id_type=MESH
        )
    for j in range(1, n):
        pl.semaphore_signal(barrier, inc=1, device_id=plane(j), device_id_type=MESH)
    pl.semaphore_signal(barrier, inc=1, device_id={"tp": 1 - core}, device_id_type=MESH)

    def send_tok(q, c, to, slot, way, kind):
        remote(
            tok.at[q, :, cols(c)], tok.at[slot, :, cols(c)],
            s_toks.at[way, kind], s_tok.at[slot, c], plane(to),
        ).start()

    def prep(q):
        ids0, ids1 = met[q, 0:1, :], met[q, 1:2, :]
        wt0, wt1 = met[q, 2:3, :], met[q, 3:4, :]
        row = lax.broadcasted_iota(jnp.int32, (rows, tokens), 0)
        e_row = (z * side + row // cap).astype(jnp.float32)
        s_row = lax.rem(row, cap).astype(jnp.float32)
        hit0 = (ids0 == e_row).astype(jnp.float32)
        hit1 = (ids1 == e_row).astype(jnp.float32)
        hit = hit0 + hit1
        before = (
            lax.broadcasted_iota(jnp.int32, (tokens, tokens), 0)
            < lax.broadcasted_iota(jnp.int32, (tokens, tokens), 1)
        ).astype(jnp.float32).astype(jnp.bfloat16)
        count = jnp.dot(hit.astype(jnp.bfloat16), before, preferred_element_type=jnp.float32)
        pick = jnp.where(count == s_row, hit, 0.0)
        sel[q] = pick.astype(jnp.bfloat16)
        w = pick * (hit0 * wt0 + hit1 * wt1)
        high = w.astype(jnp.bfloat16)
        mix[q, 0] = high
        mix[q, 1] = (w - high.astype(jnp.float32)).astype(jnp.bfloat16)

    for copy in firsts[3:]:
        copy.wait()
    met[0, 0:2, :] = ids[...].astype(jnp.float32)
    met[0, 2:4, :] = wts[...]
    met[0, 4:8, :] = jnp.zeros((4, tokens), jnp.float32)
    prep(0)
    for copy in firsts[:3]:
        copy.wait()
    slab = min(32, tokens)

    @pl.loop(0, tokens // slab)
    def _(i):
        at = pl.ds(pl.multiple_of(i * slab, slab), slab)
        v = src[at, :].astype(jnp.float32)
        v = v - jnp.mean(v, axis=-1, keepdims=True)
        spread = jnp.mean(v * v, axis=-1, keepdims=True)
        y = v * lax.rsqrt(spread + 1e-05) * gn[...] + bs[...]
        tok[0, at, :] = y.astype(jnp.bfloat16)

    pl.semaphore_wait(barrier, side - 1 + n)

    @pl.loop(0, k)
    def _(c):
        send_tok(0, c, up, 2, 0, 0)
        send_tok(0, c, back, 1, 1, 0)

    for i, (to, slot) in enumerate([(up, 2), (back, 1), (over, 3)]):
        remote(met.at[0], met.at[slot], s_mets.at[i], s_met.at[slot], plane(to)).start()

    def disp(q, c):
        y = jnp.dot(sel[q], tok[q, :, cols(c)], preferred_element_type=jnp.float32)
        snd[q, :, cols(c)] = y.astype(jnp.bfloat16)
        xin[q, band(p), cols(c)] = snd[q, band(p), cols(c)]
        for j in range(1, side):
            o = peer(j)
            remote(
                snd.at[q, band(o), cols(c)], xin.at[q, band(p), cols(c)],
                s_xs.at[q], s_x.at[q], {"ep": z * side + o},
            ).start()

    def others(ref, q):
        return ref.at[q, pl.ds(0, (side - 1) * cap)]

    tile = min(256, half)
    per = half // tile

    def gate(q, i):
        h, at = i // per, lax.rem(i, per)
        part = pl.ds(pl.multiple_of(at * tile, tile), tile)
        x = xin[q]
        g = jnp.dot(x, wg[h, :, part], preferred_element_type=jnp.float32)
        u = jnp.dot(x, wu[h, :, part], preferred_element_type=jnp.float32)
        v = g / (1.0 + jnp.exp(-g)) * u
        hid[q, :, pl.ds(pl.multiple_of(i * tile, tile), tile)] = v.astype(jnp.bfloat16)

    def gates(q):
        landed(others(xin, q), s_x.at[q])
        pl.loop(0, 2 * per)(lambda i: gate(q, i))

    def product(q, c):
        y = jnp.dot(hid[q], wd[:, cols(c)], preferred_element_type=jnp.float32)
        res[q, :, cols(c)] = y.astype(jnp.bfloat16)
        ret[q, band(p), cols(c)] = res[q, band(p), cols(c)]

    def give(q, c):
        for j in range(1, side):
            o = peer(j)
            remote(
                res.at[q, band(o), cols(c)], ret.at[q, band(p), cols(c)],
                s_rs.at[q], s_r.at[q, c], {"ep": z * side + o},
            ).start()

    def down(q, c):
        product(q, c)
        give(q, c)

    def weigh(q, c):
        landed(ret.at[q, pl.ds(0, (side - 1) * cap), cols(c)], s_r.at[q, c])
        r = ret[q, :, cols(c)]
        dims = (((0,), (0,)), ((), ()))
        return lax.dot_general(
            mix[q, 0], r, dims, preferred_element_type=jnp.float32
        ) + lax.dot_general(mix[q, 1], r, dims, preferred_element_type=jnp.float32)

    def combine(q, c, to, slot, add):
        y = weigh(q, c)
        if add:
            landed(racc.at[2, c], s_p.at[2, c])
            y = y + racc[2, c].astype(jnp.float32)
        psend[q - 1, c] = y.astype(jnp.bfloat16)
        remote(
            psend.at[q - 1, c], racc.at[slot, c], s_ps.at[q - 1], s_p.at[slot, c], plane(to)
        ).start()

    def arrived(q, c):
        landed(tok.at[q, :, cols(c)], s_tok.at[q, c])

    halfrows = pl.ds(pl.multiple_of(core * half, half), half)
    pairs = [
        (gw.at[0], wg.at[core]), (uw.at[0], wu.at[core]), (dw.at[0], wd.at[halfrows]),
    ]

    disp(0, 0)
    for i, (a, b) in enumerate(pairs):
        pltpu.make_async_copy(a, b, s_wl.at[i]).start()
        remote(a, b, s_ws.at[i], s_wr.at[i], {"tp": 1 - core}).start()
    pl.loop(1, k)(lambda c: disp(0, c))

    for q in (1, 2, 3):
        landed(met.at[q], s_met.at[q])
        prep(q)

    @pl.loop(0, HALF)
    def _(c):
        arrived(1, c)
        disp(1, c)
        arrived(2, c)
        send_tok(2, c, up, 3, 0, 1)
        disp(2, c)

    @pl.loop(HALF, k)
    def _(c):
        arrived(1, c)
        send_tok(1, c, back, 3, 1, 1)
        disp(1, c)
        arrived(2, c)
        disp(2, c)

    for i, (a, b) in enumerate(pairs):
        pltpu.make_async_copy(a, b, s_wl.at[i]).wait()
        landed(b, s_wr.at[i])
    landed(others(xin, 0), s_x.at[0])

    turns = 2 * per // HALF if 2 * per >= HALF else 1

    @pl.loop(0, HALF)
    def _(i):
        for c in (i, i + HALF):
            arrived(3, c)
            disp(3, c)
        for j in range(turns):
            gate(0, i * turns + j)

    pl.loop(0, k)(lambda c: product(0, c))
    gates(1)
    pl.loop(HALF, k)(lambda c: down(1, c))
    gates(2)
    pl.loop(0, HALF)(lambda c: down(2, c))
    gates(3)

    @pl.loop(0, HALF)
    def _(i):
        down(3, i)
        down(3, i + HALF)

    @pl.loop(0, HALF)
    def _(i):
        down(1, i)
        down(2, i + HALF)

    pl.loop(0, k)(lambda c: give(0, c))

    @pl.loop(0, HALF)
    def _(i):
        combine(1, i + HALF, up, 0, False)
        combine(2, i, back, 1, False)

    @pl.loop(0, HALF)
    def _(i):
        combine(3, i, up, 2, False)
        combine(3, i + HALF, back, 2, False)

    @pl.loop(0, HALF)
    def _(i):
        combine(1, i, up, 0, True)
        combine(2, i + HALF, back, 1, True)

    @pl.loop(0, k)
    def _(c):
        y = weigh(0, c)
        for slot in (0, 1):
            landed(racc.at[slot, c], s_p.at[slot, c])
            y = y + racc[slot, c].astype(jnp.float32)
        fin[:, cols(c)] = y.astype(out.dtype)
        pltpu.make_async_copy(fin.at[:, cols(c)], out.at[:, cols(c)], s_o.at[0]).start()

    for i, slot in enumerate((2, 1, 3)):
        landed(met.at[slot], s_mets.at[i])
    for i, (a, b) in enumerate(pairs):
        landed(b, s_ws.at[i])
    for way in range(2):
        landed(tok.at[0], s_toks.at[way, 0])
        landed(tok.at[0, :, pl.ds(0, HALF * wide)], s_toks.at[way, 1])
    for q in range(n):
        landed(others(snd, q), s_xs.at[q])
        landed(others(res, q), s_rs.at[q])
    for q in range(1, n):
        landed(psend.at[q - 1], s_ps.at[q - 1])
    pltpu.make_async_copy(fin, out, s_o.at[0]).wait()


def body(
    tokens, norm_gain, norm_bias, gate_weight, up_weight, down_weight, expert_ids, route_weights
):
    count, width = tokens.shape
    experts = lax.axis_size("ep")
    cap = max(4 * count // experts, 4)
    side = experts // LINE
    half = gate_weight.shape[2]
    rows = side * cap
    wide = width // CHUNKS
    bf = jnp.bfloat16
    dma = pltpu.SemaphoreType.DMA
    hbm = pl.BlockSpec(memory_space=pl.ANY)
    return pl.pallas_call(
        functools.partial(kernel, side),
        out_shape=jax.ShapeDtypeStruct((count, width), bf),
        in_specs=[hbm] * 8,
        out_specs=hbm,
        scratch_shapes=[
            pltpu.VMEM((count, width), bf),
            pltpu.VMEM((1, width), jnp.float32),
            pltpu.VMEM((1, width), jnp.float32),
            pltpu.VMEM((2, count), jnp.int32),
            pltpu.VMEM((2, count), jnp.float32),
            pltpu.VMEM((LINE, count, width), bf),
            pltpu.VMEM((LINE, 8, count), jnp.float32),
            pltpu.VMEM((2, width, half), bf),
            pltpu.VMEM((2, width, half), bf),
            pltpu.VMEM((2 * half, width), bf),
            pltpu.VMEM((LINE, rows, count), bf),
            pltpu.VMEM((LINE, 2, rows, count), bf),
            pltpu.VMEM((LINE, rows, width), bf),
            pltpu.VMEM((LINE, rows, width), bf),
            pltpu.VMEM((LINE, rows, 2 * half), bf),
            pltpu.VMEM((LINE, rows, width), bf),
            pltpu.VMEM((LINE, rows, width), bf),
            pltpu.VMEM((LINE - 1, CHUNKS, count, wide), bf),
            pltpu.VMEM((LINE - 1, CHUNKS, count, wide), bf),
            pltpu.VMEM((count, width), bf),
            dma((5,)),
            dma((LINE,)),
            dma((LINE - 1,)),
            dma((3,)),
            dma((3,)),
            dma((3,)),
            dma((LINE, CHUNKS)),
            dma((2, 2)),
            dma((LINE,)),
            dma((LINE,)),
            dma((LINE, CHUNKS)),
            dma((LINE,)),
            dma((LINE - 1, CHUNKS)),
            dma((LINE - 1,)),
            dma((1,)),
        ],
        compiler_params=pltpu.CompilerParams(
            collective_id=0, has_side_effects=True, vmem_limit_bytes=60 * 1024 * 1024
        ),
    )(
        tokens, norm_gain[None], norm_bias[None], expert_ids.T, route_weights.T,
        gate_weight, up_weight, down_weight,
    )


def solution(mesh):
    placed = (
        P(("ep", "tp"), None),
        P(),
        P(),
        P("ep", None, "tp"),
        P("ep", None, "tp"),
        P("ep", "tp", None),
        P(("ep", "tp"), None),
        P(("ep", "tp"), None),
    )
    return jax.shard_map(
        body, mesh=mesh, in_specs=placed, out_specs=P(("ep", "tp"), None), check_vma=False
    )
```

time: 141 us -> 120 us (0.85); the launches traced: 139 us -> 120 us
  Pallas kernels: 135 us -> 118 us
    pallas_call x1, Pallas kernels: 135 us -> 118 us  [body(): pl.pallas_call(functools.partial(kernel, side), out_shape=jax.ShapeDtypeS...]
where the time goes in v1:
time: 120 us
  Pallas kernels  118 us (98%)
  local copies, waits for them, and re-layouts  2.3 us (2%)
    pallas_call x1, Pallas kernels, body(): pl.pallas_call(functools.partial(kernel, side), out_shape=jax.ShapeDtypeS...  118 us

profile of v1, /device:TPU:0, one launch (start us, length us, event | category | flops | bytes accessed | tf_op | source)
XLA Modules:
  0.0 120.3 jit_solution(8527691823431786144)
XLA Ops:
  0.0 118.0 %shard_map.82 = bf16[256,2048]{1,0:T(8,128)(2,1)} custom-call(bf16[256,2048]{1,0:T(8,128)(2,1)} %raw.1, f32[1,2048]{1,0:T(1,128)} %bitcast.4, f32[1,2048]{1,0:T(1,128)} %bitcast.5, s32[2,256]{1,0:T(2,128)} %bitcast.6, f32[2,256]{1,0:T(2,128)} %bitcast.7, bf16[1,2048,512]{2,1,0:T(8,128)(2,1)} %gw.1, bf16[1,2048,512]{2,1,0:T(8,128)(2,1)} %uw.1, ...), custom_call_target="tpu_custom_call" | custom-call | tf_op jit(solution)/shard_map/pallas_call | solution.py:313
  118.0 2.3 %copy.10 = bf16[256,2048]{1,0:T(8,128)(2,1)} copy(bf16[256,2048]{1,0:T(8,128)(2,1)} %shard_map.82) | data formatting | bytes 2097152

commit v2 on v1

--- a/solution.py
+++ b/solution.py
@@ -15,7 +15,7 @@
 
 def kernel(
     planes, raw, gain, bias, idsin, wtin, gw, uw, dw, out,
-    src, gn, bs, ids, wts, tok, met, wg, wu, wd, sel, mix, snd, xin, hid, res, ret, psend, racc,
+    src, gn, bs, mu, rs, ids, wts, tok, met, wg, wu, wd, sel, mix, snd, xin, hid, res, ret, psend, racc,
     fin, s_own, s_met, s_mets, s_wl, s_ws, s_wr, s_tok, s_toks, s_x, s_xs, s_r, s_rs, s_p, s_ps, s_o,
 ):
     n = LINE
@@ -51,6 +51,12 @@
 
     def landed(ref, sem):
         pltpu.make_async_copy(ref, ref, sem).wait()
+
+    def step(name):
+        def run(f):
+            with jax.named_scope(name):
+                f()
+        return run
 
     firsts = [
         pltpu.make_async_copy(a, b, s_own.at[i])
@@ -96,34 +102,42 @@
         mix[q, 0] = high
         mix[q, 1] = (w - high.astype(jnp.float32)).astype(jnp.bfloat16)
 
-    for copy in firsts[3:]:
-        copy.wait()
-    met[0, 0:2, :] = ids[...].astype(jnp.float32)
-    met[0, 2:4, :] = wts[...]
-    met[0, 4:8, :] = jnp.zeros((4, tokens), jnp.float32)
-    prep(0)
-    for copy in firsts[:3]:
-        copy.wait()
+    @step("prep0")
+    def _():
+        for copy in firsts[3:]:
+            copy.wait()
+        met[0, 0:2, :] = ids[...].astype(jnp.float32)
+        met[0, 2:4, :] = wts[...]
+        met[0, 4:8, :] = jnp.zeros((4, tokens), jnp.float32)
+        prep(0)
+
+    @step("raw")
+    def _():
+        for copy in firsts[:3]:
+            copy.wait()
+
     slab = min(32, tokens)
 
-    @pl.loop(0, tokens // slab)
-    def _(i):
-        at = pl.ds(pl.multiple_of(i * slab, slab), slab)
-        v = src[at, :].astype(jnp.float32)
-        v = v - jnp.mean(v, axis=-1, keepdims=True)
-        spread = jnp.mean(v * v, axis=-1, keepdims=True)
-        y = v * lax.rsqrt(spread + 1e-05) * gn[...] + bs[...]
-        tok[0, at, :] = y.astype(jnp.bfloat16)
-
-    pl.semaphore_wait(barrier, side - 1 + n)
-
-    @pl.loop(0, k)
-    def _(c):
-        send_tok(0, c, up, 2, 0, 0)
-        send_tok(0, c, back, 1, 1, 0)
-
-    for i, (to, slot) in enumerate([(up, 2), (back, 1), (over, 3)]):
-        remote(met.at[0], met.at[slot], s_mets.at[i], s_met.at[slot], plane(to)).start()
+    @step("stats")
+    def _():
+        @pl.loop(0, tokens // slab)
+        def _(i):
+            at = pl.ds(pl.multiple_of(i * slab, slab), slab)
+            v = src[at, :].astype(jnp.float32)
+            mean = jnp.mean(v, axis=-1, keepdims=True)
+            v = v - mean
+            spread = jnp.mean(v * v, axis=-1, keepdims=True)
+            mu[at, :] = mean
+            rs[at, :] = lax.rsqrt(spread + 1e-05)
+
+    @step("meet")
+    def _():
+        pl.semaphore_wait(barrier, side - 1 + n)
+
+    @step("own")
+    def _():
+        for i, (to, slot) in enumerate([(up, 2), (back, 1), (over, 3)]):
+            remote(met.at[0], met.at[slot], s_mets.at[i], s_met.at[slot], plane(to)).start()
 
     def disp(q, c):
         y = jnp.dot(sel[q], tok[q, :, cols(c)], preferred_element_type=jnp.float32)
@@ -152,7 +166,6 @@
         hid[q, :, pl.ds(pl.multiple_of(i * tile, tile), tile)] = v.astype(jnp.bfloat16)
 
     def gates(q):
-        landed(others(xin, q), s_x.at[q])
         pl.loop(0, 2 * per)(lambda i: gate(q, i))
 
     def product(q, c):
@@ -173,7 +186,6 @@
         give(q, c)
 
     def weigh(q, c):
-        landed(ret.at[q, pl.ds(0, (side - 1) * cap), cols(c)], s_r.at[q, c])
         r = ret[q, :, cols(c)]
         dims = (((0,), (0,)), ((), ()))
         return lax.dot_general(
@@ -181,6 +193,7 @@
         ) + lax.dot_general(mix[q, 1], r, dims, preferred_element_type=jnp.float32)
 
     def combine(q, c, to, slot, add):
+        landed(ret.at[q, pl.ds(0, (side - 1) * cap), cols(c)], s_r.at[q, c])
         y = weigh(q, c)
         if add:
             landed(racc.at[2, c], s_p.at[2, c])
@@ -198,89 +211,153 @@
         (gw.at[0], wg.at[core]), (uw.at[0], wu.at[core]), (dw.at[0], wd.at[halfrows]),
     ]
 
-    disp(0, 0)
-    for i, (a, b) in enumerate(pairs):
-        pltpu.make_async_copy(a, b, s_wl.at[i]).start()
-        remote(a, b, s_ws.at[i], s_wr.at[i], {"tp": 1 - core}).start()
-    pl.loop(1, k)(lambda c: disp(0, c))
-
-    for q in (1, 2, 3):
-        landed(met.at[q], s_met.at[q])
-        prep(q)
-
-    @pl.loop(0, HALF)
-    def _(c):
-        arrived(1, c)
-        disp(1, c)
-        arrived(2, c)
-        send_tok(2, c, up, 3, 0, 1)
-        disp(2, c)
-
-    @pl.loop(HALF, k)
-    def _(c):
-        arrived(1, c)
-        send_tok(1, c, back, 3, 1, 1)
-        disp(1, c)
-        arrived(2, c)
-        disp(2, c)
-
-    for i, (a, b) in enumerate(pairs):
-        pltpu.make_async_copy(a, b, s_wl.at[i]).wait()
-        landed(b, s_wr.at[i])
-    landed(others(xin, 0), s_x.at[0])
+    def first(c):
+        v = (src[:, cols(c)].astype(jnp.float32) - mu[...]) * rs[...]
+        tok[0, :, cols(c)] = (v * gn[:, cols(c)] + bs[:, cols(c)]).astype(jnp.bfloat16)
+        send_tok(0, c, up, 2, 0, 0)
+        send_tok(0, c, back, 1, 1, 0)
+        disp(0, c)
+
+    @step("disp0")
+    def _():
+        first(0)
+        for i, (a, b) in enumerate(pairs):
+            pltpu.make_async_copy(a, b, s_wl.at[i]).start()
+            remote(a, b, s_ws.at[i], s_wr.at[i], {"tp": 1 - core}).start()
+        pl.loop(1, k)(first)
+
+    @step("preps")
+    def _():
+        for q in (1, 2, 3):
+            landed(met.at[q], s_met.at[q])
+            prep(q)
+
+    @step("disp12a")
+    def _():
+        @pl.loop(0, HALF)
+        def _(c):
+            arrived(1, c)
+            disp(1, c)
+            arrived(2, c)
+            send_tok(2, c, up, 3, 0, 1)
+            disp(2, c)
+
+    @step("disp12b")
+    def _():
+        @pl.loop(HALF, k)
+        def _(c):
+            arrived(1, c)
+            send_tok(1, c, back, 3, 1, 1)
+            disp(1, c)
+            arrived(2, c)
+            disp(2, c)
+
+    @step("weights")
+    def _():
+        for i, (a, b) in enumerate(pairs):
+            pltpu.make_async_copy(a, b, s_wl.at[i]).wait()
+            landed(b, s_wr.at[i])
+
+    @step("in0")
+    def _():
+        landed(others(xin, 0), s_x.at[0])
 
     turns = 2 * per // HALF if 2 * per >= HALF else 1
 
-    @pl.loop(0, HALF)
-    def _(i):
-        for c in (i, i + HALF):
-            arrived(3, c)
-            disp(3, c)
-        for j in range(turns):
-            gate(0, i * turns + j)
-
-    pl.loop(0, k)(lambda c: product(0, c))
-    gates(1)
-    pl.loop(HALF, k)(lambda c: down(1, c))
-    gates(2)
-    pl.loop(0, HALF)(lambda c: down(2, c))
-    gates(3)
-
-    @pl.loop(0, HALF)
-    def _(i):
-        down(3, i)
-        down(3, i + HALF)
-
-    @pl.loop(0, HALF)
-    def _(i):
-        down(1, i)
-        down(2, i + HALF)
-
-    pl.loop(0, k)(lambda c: give(0, c))
-
-    @pl.loop(0, HALF)
-    def _(i):
-        combine(1, i + HALF, up, 0, False)
-        combine(2, i, back, 1, False)
-
-    @pl.loop(0, HALF)
-    def _(i):
-        combine(3, i, up, 2, False)
-        combine(3, i + HALF, back, 2, False)
-
-    @pl.loop(0, HALF)
-    def _(i):
-        combine(1, i, up, 0, True)
-        combine(2, i + HALF, back, 1, True)
-
-    @pl.loop(0, k)
-    def _(c):
-        y = weigh(0, c)
-        for slot in (0, 1):
-            landed(racc.at[slot, c], s_p.at[slot, c])
-            y = y + racc[slot, c].astype(jnp.float32)
-        fin[:, cols(c)] = y.astype(out.dtype)
-        pltpu.make_async_copy(fin.at[:, cols(c)], out.at[:, cols(c)], s_o.at[0]).start()
+    @step("disp3gate0")
+    def _():
+        @pl.loop(0, HALF)
+        def _(i):
+            for c in (i, i + HALF):
+                arrived(3, c)
+                disp(3, c)
+            for j in range(turns):
+                gate(0, i * turns + j)
+
+    @step("product0")
+    def _():
+        pl.loop(0, k)(lambda c: product(0, c))
+
+    @step("in1")
+    def _():
+        landed(others(xin, 1), s_x.at[1])
+
+    @step("gates1")
+    def _():
+        gates(1)
+
+    @step("down1")
+    def _():
+        pl.loop(HALF, k)(lambda c: down(1, c))
+
+    @step("in2")
+    def _():
+        landed(others(xin, 2), s_x.at[2])
+
+    @step("gates2")
+    def _():
+        gates(2)
+
+    @step("down2")
+    def _():
+        pl.loop(0, HALF)(lambda c: down(2, c))
+
+    @step("in3")
+    def _():
+        landed(others(xin, 3), s_x.at[3])
+
+    @step("gates3")
+    def _():
+        gates(3)
+
+    @step("down3")
+    def _():
+        @pl.loop(0, HALF)
+        def _(i):
+            down(3, i)
+            down(3, i + HALF)
+            combine(1, i + HALF, up, 0, False)
+            combine(2, i, back, 1, False)
+
+    @step("down12")
+    def _():
+        @pl.loop(0, HALF)
+        def _(i):
+            down(1, i)
+            down(2, i + HALF)
+
+    @step("give0")
+    def _():
+        pl.loop(0, k)(lambda c: give(0, c))
+
+    @step("comb3")
+    def _():
+        @pl.loop(0, HALF)
+        def _(i):
+            combine(3, i, up, 2, False)
+            combine(3, i + HALF, back, 2, False)
+
+    @step("comb12b")
+    def _():
+        @pl.loop(0, HALF)
+        def _(i):
+            combine(1, i, up, 0, True)
+            combine(2, i + HALF, back, 1, True)
+
+    @step("last")
+    def _():
+        @pl.loop(0, k)
+        def _(c):
+            with jax.named_scope("wr"):
+                landed(ret.at[0, pl.ds(0, (side - 1) * cap), cols(c)], s_r.at[0, c])
+            with jax.named_scope("wp"):
+                for slot in (0, 1):
+                    landed(racc.at[slot, c], s_p.at[slot, c])
+            y = weigh(0, c)
+            for slot in (0, 1):
+                y = y + racc[slot, c].astype(jnp.float32)
+            fin[:, cols(c)] = y.astype(out.dtype)
+            pltpu.make_async_copy(fin.at[:, cols(c)], out.at[:, cols(c)], s_o.at[0]).start()
 
     for i, slot in enumerate((2, 1, 3)):
         landed(met.at[slot], s_mets.at[i])
@@ -319,6 +396,8 @@
             pltpu.VMEM((count, width), bf),
             pltpu.VMEM((1, width), jnp.float32),
             pltpu.VMEM((1, width), jnp.float32),
+            pltpu.VMEM((count, 1), jnp.float32),
+            pltpu.VMEM((count, 1), jnp.float32),
             pltpu.VMEM((2, count), jnp.int32),
             pltpu.VMEM((2, count), jnp.float32),
             pltpu.VMEM((LINE, count, width), bf),

time: 120 us -> 105 us (0.88)
  Pallas kernels: 118 us -> 102 us
    pallas_call x1, Pallas kernels: 118 us -> 102 us  [body(): pl.pallas_call(functools.partial(kernel, side), out_shape=jax.ShapeDtypeS...]
where the time goes in v2:
time: 105 us
  Pallas kernels  102 us (97%)
  local copies, waits for them, and re-layouts  2.3 us (2%)
    pallas_call x1, Pallas kernels, body(): pl.pallas_call(functools.partial(kernel, side), out_shape=jax.ShapeDtypeS...  102 us
    unnamed x1, local copies, waits for them, and re-layouts  2.3 us

profile of v2, /device:TPU:0, one launch (start us, length us, event | category | flops | bytes accessed | tf_op | source)
XLA Modules:
  0.0 104.6 jit_solution(3537476413231049685)
XLA Ops:
  0.0 102.3 %shard_map.82 = bf16[256,2048]{1,0:T(8,128)(2,1)} custom-call(bf16[256,2048]{1,0:T(8,128)(2,1)} %raw.1, f32[1,2048]{1,0:T(1,128)} %bitcast.4, f32[1,2048]{1,0:T(1,128)} %bitcast.5, s32[2,256]{1,0:T(2,128)} %bitcast.6, f32[2,256]{1,0:T(2,128)} %bitcast.7, bf16[1,2048,512]{2,1,0:T(8,128)(2,1)} %gw.1, bf16[1,2048,512]{2,1,0:T(8,128)(2,1)} %uw.1, ...), custom_call_target="tpu_custom_call" | custom-call | tf_op jit(solution)/shard_map/pallas_call | solution.py:390
  102.3 2.3 %copy.10 = bf16[256,2048]{1,0:T(8,128)(2,1)} copy(bf16[256,2048]{1,0:T(8,128)(2,1)} %shard_map.82) | data formatting | bytes 2097152

commit v3 on v2

--- a/solution.py
+++ b/solution.py
@@ -15,8 +15,8 @@
 
 def kernel(
     planes, raw, gain, bias, idsin, wtin, gw, uw, dw, out,
-    src, gn, bs, mu, rs, ids, wts, tok, met, wg, wu, wd, sel, mix, snd, xin, hid, res, ret, psend, racc,
-    fin, s_own, s_met, s_mets, s_wl, s_ws, s_wr, s_tok, s_toks, s_x, s_xs, s_r, s_rs, s_p, s_ps, s_o,
+    src, gn, bs, part, mu, rs, ids, wts, tok, met, wg, wu, wd, sel, mix, snd, xin, hid, res, ret, psend, racc,
+    s_own, s_met, s_mets, s_wl, s_ws, s_wr, s_tok, s_toks, s_x, s_xs, s_r, s_rs, s_p, s_ps,
 ):
     n = LINE
     side = planes
@@ -117,18 +117,29 @@
             copy.wait()
 
     slab = min(32, tokens)
+    lanes = part.shape[1]
 
     @step("stats")
     def _():
-        @pl.loop(0, tokens // slab)
-        def _(i):
+        def total(i, f):
             at = pl.ds(pl.multiple_of(i * slab, slab), slab)
-            v = src[at, :].astype(jnp.float32)
-            mean = jnp.mean(v, axis=-1, keepdims=True)
-            v = v - mean
-            spread = jnp.mean(v * v, axis=-1, keepdims=True)
-            mu[at, :] = mean
-            rs[at, :] = lax.rsqrt(spread + 1e-05)
+            parts = [
+                f(src[at, j * lanes : (j + 1) * lanes].astype(jnp.float32), at)
+                for j in range(width // lanes)
+            ]
+            while len(parts) > 1:
+                parts = [a + b for a, b in zip(parts[::2], parts[1::2])]
+            part[at, :] = parts[0]
+
+        pl.loop(0, tokens // slab)(lambda i: total(i, lambda v, at: v))
+        mu[...] = jnp.sum(part[...], axis=-1, keepdims=True) / width
+
+        def square(v, at):
+            v = v - mu[at, :]
+            return v * v
+
+        pl.loop(0, tokens // slab)(lambda i: total(i, square))
+        rs[...] = lax.rsqrt(jnp.sum(part[...], axis=-1, keepdims=True) / width + 1e-05)
 
     @step("meet")
     def _():
@@ -344,6 +355,20 @@
             combine(1, i, up, 0, True)
             combine(2, i + HALF, back, 1, True)
 
+    @step("drain")
+    def _():
+        for i, slot in enumerate((2, 1, 3)):
+            landed(met.at[slot], s_mets.at[i])
+        for i, (a, b) in enumerate(pairs):
+            landed(b, s_ws.at[i])
+        for way in range(2):
+            landed(tok.at[0], s_toks.at[way, 0])
+            landed(tok.at[0, :, pl.ds(0, HALF * wide)], s_toks.at[way, 1])
+        for q in range(n):
+            landed(others(snd, q), s_xs.at[q])
+        for q in range(1, n):
+            landed(others(res, q), s_rs.at[q])
+
     @step("last")
     def _():
         @pl.loop(0, k)
@@ -356,22 +381,13 @@
             y = weigh(0, c)
             for slot in (0, 1):
                 y = y + racc[slot, c].astype(jnp.float32)
-            fin[:, cols(c)] = y.astype(out.dtype)
-            pltpu.make_async_copy(fin.at[:, cols(c)], out.at[:, cols(c)], s_o.at[0]).start()
-
-    for i, slot in enumerate((2, 1, 3)):
-        landed(met.at[slot], s_mets.at[i])
-    for i, (a, b) in enumerate(pairs):
-        landed(b, s_ws.at[i])
-    for way in range(2):
-        landed(tok.at[0], s_toks.at[way, 0])
-        landed(tok.at[0, :, pl.ds(0, HALF * wide)], s_toks.at[way, 1])
-    for q in range(n):
-        landed(others(snd, q), s_xs.at[q])
-        landed(others(res, q), s_rs.at[q])
-    for q in range(1, n):
-        landed(psend.at[q - 1], s_ps.at[q - 1])
-    pltpu.make_async_copy(fin, out, s_o.at[0]).wait()
+            out[:, cols(c)] = y.astype(out.dtype)
+
+    @step("end")
+    def _():
+        for q in range(1, n):
+            landed(psend.at[q - 1], s_ps.at[q - 1])
+        landed(others(res, 0), s_rs.at[0])
 
 
 def body(
@@ -389,13 +405,14 @@
     hbm = pl.BlockSpec(memory_space=pl.ANY)
     return pl.pallas_call(
         functools.partial(kernel, side),
-        out_shape=jax.ShapeDtypeStruct((count, width), bf),
+        out_shape=pltpu.VMEM((count, width), bf),
         in_specs=[hbm] * 8,
-        out_specs=hbm,
+        out_specs=pl.BlockSpec(memory_space=pltpu.VMEM),
         scratch_shapes=[
             pltpu.VMEM((count, width), bf),
             pltpu.VMEM((1, width), jnp.float32),
             pltpu.VMEM((1, width), jnp.float32),
+            pltpu.VMEM((count, 128), jnp.float32),
             pltpu.VMEM((count, 1), jnp.float32),
             pltpu.VMEM((count, 1), jnp.float32),
             pltpu.VMEM((2, count), jnp.int32),
@@ -414,7 +431,6 @@
             pltpu.VMEM((LINE, rows, width), bf),
             pltpu.VMEM((LINE - 1, CHUNKS, count, wide), bf),
             pltpu.VMEM((LINE - 1, CHUNKS, count, wide), bf),
-            pltpu.VMEM((count, width), bf),
             dma((5,)),
             dma((LINE,)),
             dma((LINE - 1,)),
@@ -429,14 +445,18 @@
             dma((LINE,)),
             dma((LINE - 1, CHUNKS)),
             dma((LINE - 1,)),
-            dma((1,)),
         ],
         compiler_params=pltpu.CompilerParams(
-            collective_id=0, has_side_effects=True, vmem_limit_bytes=60 * 1024 * 1024
+            collective_id=0, has_side_effects=True, vmem_limit_bytes=52 * 1024 * 1024
         ),
     )(
-        tokens, norm_gain[None], norm_bias[None], expert_ids.T, route_weights.T,
-        gate_weight, up_weight, down_weight,
+        *[
+            pltpu.with_memory_space_constraint(a, pltpu.HBM)
+            for a in (
+                tokens, norm_gain[None], norm_bias[None], expert_ids.T, route_weights.T,
+                gate_weight, up_weight, down_weight,
+            )
+        ]
     )
 
 

time: 105 us -> 103 us (0.981)
  local copies, waits for them, and re-layouts: 2.3 us -> 0.97 us
    unnamed x1, local copies, waits for them, and re-layouts: 2.3 us -> 0.97 us
where the time goes in v3:
time: 103 us
  Pallas kernels  102 us (99%)
    pallas_call x1, Pallas kernels, body(): pl.pallas_call(functools.partial(kernel, side), out_shape=pltpu.VMEM((cou...  102 us

profile of v3, /device:TPU:0, one launch (start us, length us, event | category | flops | bytes accessed | tf_op | source)
XLA Modules:
  0.0 102.6 jit_solution(7607817816291998475)
XLA Ops:
  0.0 101.6 %shard_map.82 = bf16[256,2048]{1,0:T(8,128)(2,1)S(1)} custom-call(bf16[256,2048]{1,0:T(8,128)(2,1)} %raw.1, f32[1,2048]{1,0:T(1,128)} %bitcast.4, f32[1,2048]{1,0:T(1,128)} %bitcast.5, s32[2,256]{1,0:T(2,128)} %bitcast.6, f32[2,256]{1,0:T(2,128)} %bitcast.7, bf16[1,2048,512]{2,1,0:T(8,128)(2,1)} %gw.1, bf16[1,2048,512]{2,1,0:T(8,128)(2,1)} %uw.1, ...), custom_call_target="tpu_custom_call" | custom-call | tf_op jit(solution)/shard_map/pallas_call | solution.py:406
  101.6 1.0 copy.10

commit v4 on v3

--- a/solution.py
+++ b/solution.py
@@ -11,12 +11,13 @@
 LINE = 4
 CHUNKS = 8
 HALF = CHUNKS // 2
+EARLY = 2
 
 
 def kernel(
     planes, raw, gain, bias, idsin, wtin, gw, uw, dw, out,
     src, gn, bs, part, mu, rs, ids, wts, tok, met, wg, wu, wd, sel, mix, snd, xin, hid, res, ret, psend, racc,
-    s_own, s_met, s_mets, s_wl, s_ws, s_wr, s_tok, s_toks, s_x, s_xs, s_r, s_rs, s_p, s_ps,
+    s_own, s_met, s_w, s_ws, s_tok, s_toks, s_x, s_xs, s_r, s_rs, s_p, s_ps,
 ):
     n = LINE
     side = planes
@@ -40,8 +41,16 @@
 
     up, over, back = 1, 2, n - 1
 
-    def peer(j):
-        return lax.rem(p + j, side)
+    y, x = p // n, lax.rem(p, n)
+
+    def away(d):
+        return sum(min(j, n - j) for j in d)
+
+    offsets = [(b, c) for b in range(n) for c in range(n) if b or c]
+    peers = [
+        lax.rem(y + b, n) * n + lax.rem(x + c, n)
+        for b, c in sorted(offsets, key=lambda d: -away(d))
+    ]
 
     def remote(src, dst, send, recv, where):
         return pltpu.make_async_remote_copy(
@@ -67,18 +76,17 @@
     for copy in firsts:
         copy.start()
     barrier = pltpu.get_barrier_semaphore()
-    for j in range(1, side):
-        pl.semaphore_signal(
-            barrier, inc=1, device_id={"ep": z * side + peer(j)}, device_id_type=MESH
-        )
+    for o in peers:
+        pl.semaphore_signal(barrier, inc=1, device_id={"ep": z * side + o}, device_id_type=MESH)
     for j in range(1, n):
         pl.semaphore_signal(barrier, inc=1, device_id=plane(j), device_id_type=MESH)
     pl.semaphore_signal(barrier, inc=1, device_id={"tp": 1 - core}, device_id_type=MESH)
 
-    def send_tok(q, c, to, slot, way, kind):
+    def send_tok(q, c, to, slot):
+        count = k + lax.rem(c, HALF) if slot == 3 else c
         remote(
             tok.at[q, :, cols(c)], tok.at[slot, :, cols(c)],
-            s_toks.at[way, kind], s_tok.at[slot, c], plane(to),
+            s_toks.at[0], s_tok.at[count], plane(to),
         ).start()
 
     def prep(q):
@@ -141,25 +149,40 @@
         pl.loop(0, tokens // slab)(lambda i: total(i, square))
         rs[...] = lax.rsqrt(jnp.sum(part[...], axis=-1, keepdims=True) / width + 1e-05)
 
-    @step("meet")
-    def _():
-        pl.semaphore_wait(barrier, side - 1 + n)
-
-    @step("own")
-    def _():
-        for i, (to, slot) in enumerate([(up, 2), (back, 1), (over, 3)]):
-            remote(met.at[0], met.at[slot], s_mets.at[i], s_met.at[slot], plane(to)).start()
-
-    def disp(q, c):
-        y = jnp.dot(sel[q], tok[q, :, cols(c)], preferred_element_type=jnp.float32)
-        snd[q, :, cols(c)] = y.astype(jnp.bfloat16)
+    def fresh(c):
+        v = (src[:, cols(c)].astype(jnp.float32) - mu[...]) * rs[...]
+        tok[0, :, cols(c)] = (v * gn[:, cols(c)] + bs[:, cols(c)]).astype(jnp.bfloat16)
+
+    def select(q, c):
+        v = jnp.dot(sel[q], tok[q, :, cols(c)], preferred_element_type=jnp.float32)
+        snd[q, :, cols(c)] = v.astype(jnp.bfloat16)
         xin[q, band(p), cols(c)] = snd[q, band(p), cols(c)]
-        for j in range(1, side):
-            o = peer(j)
+
+    def ship(q, c):
+        for o in peers:
             remote(
                 snd.at[q, band(o), cols(c)], xin.at[q, band(p), cols(c)],
-                s_xs.at[q], s_x.at[q], {"ep": z * side + o},
+                s_xs.at[0], s_x.at[q], {"ep": z * side + o},
             ).start()
+
+    def disp(q, c):
+        select(q, c)
+        ship(q, c)
+
+    @step("early")
+    def _():
+        for c in range(EARLY):
+            fresh(c)
+            select(0, c)
+
+    @step("meet")
+    def _():
+        pl.semaphore_wait(barrier, side - 1 + n)
+
+    @step("own")
+    def _():
+        for to, slot in [(up, 2), (back, 1), (over, 3)]:
+            remote(met.at[0], met.at[slot], s_met.at[0], s_met.at[1], plane(to)).start()
 
     def others(ref, q):
         return ref.at[q, pl.ds(0, (side - 1) * cap)]
@@ -184,12 +207,18 @@
         res[q, :, cols(c)] = y.astype(jnp.bfloat16)
         ret[q, band(p), cols(c)] = res[q, band(p), cols(c)]
 
+    def pick(q, c):
+        if q == 0:
+            return c
+        if q == 3:
+            return k + lax.rem(c, HALF)
+        return k + HALF + lax.rem(c + (HALF if q == 1 else 0), k)
+
     def give(q, c):
-        for j in range(1, side):
-            o = peer(j)
+        for o in peers:
             remote(
                 res.at[q, band(o), cols(c)], ret.at[q, band(p), cols(c)],
-                s_rs.at[q], s_r.at[q, c], {"ep": z * side + o},
+                s_rs.at[0], s_r.at[pick(q, c)], {"ep": z * side + o},
             ).start()
 
     def down(q, c):
@@ -204,70 +233,75 @@
         ) + lax.dot_general(mix[q, 1], r, dims, preferred_element_type=jnp.float32)
 
     def combine(q, c, to, slot, add):
-        landed(ret.at[q, pl.ds(0, (side - 1) * cap), cols(c)], s_r.at[q, c])
-        y = weigh(q, c)
+        v = weigh(q, c)
         if add:
-            landed(racc.at[2, c], s_p.at[2, c])
-            y = y + racc[2, c].astype(jnp.float32)
-        psend[q - 1, c] = y.astype(jnp.bfloat16)
+            v = v + racc[2, c].astype(jnp.float32)
+        psend[q - 1, c] = v.astype(jnp.bfloat16)
+        count = k + lax.rem(c, HALF) if slot == 2 else c
         remote(
-            psend.at[q - 1, c], racc.at[slot, c], s_ps.at[q - 1], s_p.at[slot, c], plane(to)
+            psend.at[q - 1, c], racc.at[slot, c], s_ps.at[0], s_p.at[count], plane(to)
         ).start()
 
-    def arrived(q, c):
-        landed(tok.at[q, :, cols(c)], s_tok.at[q, c])
+    def back_in(q, c):
+        landed(ret.at[q, pl.ds(0, (side - 1) * cap), pl.ds(0, 2 * wide)], s_r.at[pick(q, c)])
+
+    def summed(i):
+        landed(racc.at[0, pl.ds(0, 2)], s_p.at[i])
+
+    def arrived(i):
+        landed(tok.at[1, :, pl.ds(0, 2 * wide)], s_tok.at[i])
 
     halfrows = pl.ds(pl.multiple_of(core * half, half), half)
     pairs = [
         (gw.at[0], wg.at[core]), (uw.at[0], wu.at[core]), (dw.at[0], wd.at[halfrows]),
     ]
 
+    def spread(c):
+        send_tok(0, c, up, 2)
+        send_tok(0, c, back, 1)
+        ship(0, c)
+
     def first(c):
-        v = (src[:, cols(c)].astype(jnp.float32) - mu[...]) * rs[...]
-        tok[0, :, cols(c)] = (v * gn[:, cols(c)] + bs[:, cols(c)]).astype(jnp.bfloat16)
-        send_tok(0, c, up, 2, 0, 0)
-        send_tok(0, c, back, 1, 1, 0)
-        disp(0, c)
+        fresh(c)
+        select(0, c)
+        spread(c)
 
     @step("disp0")
     def _():
-        first(0)
+        pl.loop(0, EARLY)(spread)
         for i, (a, b) in enumerate(pairs):
-            pltpu.make_async_copy(a, b, s_wl.at[i]).start()
-            remote(a, b, s_ws.at[i], s_wr.at[i], {"tp": 1 - core}).start()
-        pl.loop(1, k)(first)
+            pltpu.make_async_copy(a, b, s_w.at[i]).start()
+            remote(a, b, s_ws.at[i // 2], s_w.at[i], {"tp": 1 - core}).start()
+        pl.loop(EARLY, k)(first)
 
     @step("preps")
     def _():
+        landed(met.at[pl.ds(1, n - 1)], s_met.at[1])
         for q in (1, 2, 3):
-            landed(met.at[q], s_met.at[q])
             prep(q)
 
     @step("disp12a")
     def _():
         @pl.loop(0, HALF)
         def _(c):
-            arrived(1, c)
+            arrived(c)
+            send_tok(2, c, up, 3)
             disp(1, c)
-            arrived(2, c)
-            send_tok(2, c, up, 3, 0, 1)
             disp(2, c)
 
     @step("disp12b")
     def _():
         @pl.loop(HALF, k)
         def _(c):
-            arrived(1, c)
-            send_tok(1, c, back, 3, 1, 1)
+            arrived(c)
+            send_tok(1, c, back, 3)
             disp(1, c)
-            arrived(2, c)
             disp(2, c)
 
     @step("weights")
     def _():
-        for i, (a, b) in enumerate(pairs):
-            pltpu.make_async_copy(a, b, s_wl.at[i]).wait()
-            landed(b, s_wr.at[i])
+        for i, ref in enumerate((wg, wu, wd)):
+            landed(ref, s_w.at[i])
 
     @step("in0")
     def _():
@@ -279,8 +313,8 @@
     def _():
         @pl.loop(0, HALF)
         def _(i):
+            arrived(k + i)
             for c in (i, i + HALF):
-                arrived(3, c)
                 disp(3, c)
             for j in range(turns):
                 gate(0, i * turns + j)
@@ -327,6 +361,7 @@
         def _(i):
             down(3, i)
             down(3, i + HALF)
+            back_in(2, i)
             combine(1, i + HALF, up, 0, False)
             combine(2, i, back, 1, False)
 
@@ -345,6 +380,7 @@
     def _():
         @pl.loop(0, HALF)
         def _(i):
+            back_in(3, i)
             combine(3, i, up, 2, False)
             combine(3, i + HALF, back, 2, False)
 
@@ -352,32 +388,27 @@
     def _():
         @pl.loop(0, HALF)
         def _(i):
+            back_in(1, i)
+            summed(k + i)
             combine(1, i, up, 0, True)
             combine(2, i + HALF, back, 1, True)
 
     @step("drain")
     def _():
-        for i, slot in enumerate((2, 1, 3)):
-            landed(met.at[slot], s_mets.at[i])
-        for i, (a, b) in enumerate(pairs):
-            landed(b, s_ws.at[i])
-        for way in range(2):
-            landed(tok.at[0], s_toks.at[way, 0])
-            landed(tok.at[0, :, pl.ds(0, HALF * wide)], s_toks.at[way, 1])
-        for q in range(n):
-            landed(others(snd, q), s_xs.at[q])
-        for q in range(1, n):
-            landed(others(res, q), s_rs.at[q])
+        landed(met.at[pl.ds(1, n - 1)], s_met.at[0])
+        landed(wg, s_ws.at[0])
+        landed(wd.at[halfrows], s_ws.at[1])
+        landed(tok.at[pl.ds(0, n - 1)], s_toks.at[0])
+        landed(snd.at[:, pl.ds(0, (side - 1) * cap)], s_xs.at[0])
 
     @step("last")
     def _():
         @pl.loop(0, k)
         def _(c):
             with jax.named_scope("wr"):
-                landed(ret.at[0, pl.ds(0, (side - 1) * cap), cols(c)], s_r.at[0, c])
+                landed(ret.at[0, pl.ds(0, (side - 1) * cap), cols(c)], s_r.at[pick(0, c)])
             with jax.named_scope("wp"):
-                for slot in (0, 1):
-                    landed(racc.at[slot, c], s_p.at[slot, c])
+                summed(c)
             y = weigh(0, c)
             for slot in (0, 1):
                 y = y + racc[slot, c].astype(jnp.float32)
@@ -385,9 +416,8 @@
 
     @step("end")
     def _():
-        for q in range(1, n):
-            landed(psend.at[q - 1], s_ps.at[q - 1])
-        landed(others(res, 0), s_rs.at[0])
+        landed(psend, s_ps.at[0])
+        landed(res.at[:, pl.ds(0, (side - 1) * cap)], s_rs.at[0])
 
 
 def body(
@@ -432,19 +462,17 @@
             pltpu.VMEM((LINE - 1, CHUNKS, count, wide), bf),
             pltpu.VMEM((LINE - 1, CHUNKS, count, wide), bf),
             dma((5,)),
+            dma((2,)),
+            dma((3,)),
+            dma((2,)),
+            dma((CHUNKS + HALF,)),
+            dma((1,)),
             dma((LINE,)),
-            dma((LINE - 1,)),
-            dma((3,)),
-            dma((3,)),
-            dma((3,)),
-            dma((LINE, CHUNKS)),
-            dma((2, 2)),
-            dma((LINE,)),
-            dma((LINE,)),
-            dma((LINE, CHUNKS)),
-            dma((LINE,)),
-            dma((LINE - 1, CHUNKS)),
-            dma((LINE - 1,)),
+            dma((1,)),
+            dma((2 * CHUNKS + HALF,)),
+            dma((1,)),
+            dma((CHUNKS + HALF,)),
+            dma((1,)),
         ],
         compiler_params=pltpu.CompilerParams(
             collective_id=0, has_side_effects=True, vmem_limit_bytes=52 * 1024 * 1024

time: 103 us -> 101 us (0.981)
  Pallas kernels: 102 us -> 100 us
    pallas_call x1, Pallas kernels: 102 us -> 100 us  [body(): pl.pallas_call(functools.partial(kernel, side), out_shape=pltpu.VMEM((cou...]
where the time goes in v4:
time: 101 us
  Pallas kernels  100 us (99%)
    pallas_call x1, Pallas kernels, body(): pl.pallas_call(functools.partial(kernel, side), out_shape=pltpu.VMEM((cou...  100 us

profile of v4, /device:TPU:0, one launch (start us, length us, event | category | flops | bytes accessed | tf_op | source)
XLA Modules:
  0.0 101.4 jit_solution(2075211710327363924)
XLA Ops:
  0.0 100.4 %shard_map.82 = bf16[256,2048]{1,0:T(8,128)(2,1)S(1)} custom-call(bf16[256,2048]{1,0:T(8,128)(2,1)} %raw.1, f32[1,2048]{1,0:T(1,128)} %bitcast.4, f32[1,2048]{1,0:T(1,128)} %bitcast.5, s32[2,256]{1,0:T(2,128)} %bitcast.6, f32[2,256]{1,0:T(2,128)} %bitcast.7, bf16[1,2048,512]{2,1,0:T(8,128)(2,1)} %gw.1, bf16[1,2048,512]{2,1,0:T(8,128)(2,1)} %uw.1, ...), custom_call_target="tpu_custom_call" | custom-call | tf_op jit(solution)/shard_map/pallas_call | solution.py:436
  100.4 1.0 copy.10

commit v5 on v4

--- a/solution.py
+++ b/solution.py
@@ -12,6 +12,10 @@
 CHUNKS = 8
 HALF = CHUNKS // 2
 EARLY = 2
+X, Y, Z = 0, 1, 2
+SIDEWAYS = [(0, X), (1, Y)]
+SPLIT = len(SIDEWAYS)
+MIDDLE = (SPLIT + CHUNKS) // 2
 
 
 def kernel(
@@ -23,6 +27,7 @@
     side = planes
     me, core = lax.axis_index("ep"), lax.axis_index("tp")
     z, p = me // side, lax.rem(me, side)
+    y, x = p // LINE, lax.rem(p, LINE)
     tokens, width = raw.shape
     half = gw.shape[2]
     rows = snd.shape[1]
@@ -40,8 +45,20 @@
         return {"ep": lax.rem(z + j, n) * side + p}
 
     up, over, back = 1, 2, n - 1
-
-    y, x = p // n, lax.rem(p, n)
+    role = {0: 0, up: 1, back: 2, over: 3}
+    steps = {q: j for j, q in role.items()}
+
+    def ident(a, b, c):
+        return {"ep": a * side + b * n + c}
+
+    def turn(a, j):
+        return lax.rem(a + j, n) if j else a
+
+    def ring(way, j):
+        return ident(
+            turn(z, j if way == Z else 0), turn(y, j if way == Y else 0), turn(x, j if way == X else 0)
+        )
+
 
     def away(d):
         return sum(min(j, n - j) for j in d)
@@ -82,18 +99,31 @@
         pl.semaphore_signal(barrier, inc=1, device_id=plane(j), device_id_type=MESH)
     pl.semaphore_signal(barrier, inc=1, device_id={"tp": 1 - core}, device_id_type=MESH)
 
-    def send_tok(q, c, to, slot):
-        count = k + lax.rem(c, HALF) if slot == 3 else c
+    def send_tok(way, q, c, to, slot, part=None):
+        if slot < 3:
+            count = c
+        elif way == Z:
+            count = k + SPLIT + lax.rem(c - SPLIT, MIDDLE - SPLIT)
+        else:
+            count = k + c
+        at = cols(c)
+        if part is not None:
+            at = pl.ds(c * wide + part * (wide // 2), wide // 2)
         remote(
-            tok.at[q, :, cols(c)], tok.at[slot, :, cols(c)],
-            s_toks.at[0], s_tok.at[count], plane(to),
+            tok.at[q, :, at], tok.at[slot, :, at], s_toks.at[0], s_tok.at[count], ring(way, to)
         ).start()
 
-    def prep(q):
-        ids0, ids1 = met[q, 0:1, :], met[q, 1:2, :]
-        wt0, wt1 = met[q, 2:3, :], met[q, 3:4, :]
+    def prep(way, q):
+        at = (way, q) if q else (Z, 0)
+        ids0, ids1 = met[at + (slice(0, 1),)], met[at + (slice(1, 2),)]
+        wt0, wt1 = met[at + (slice(2, 3),)], met[at + (slice(3, 4),)]
         row = lax.broadcasted_iota(jnp.int32, (rows, tokens), 0)
-        e_row = (z * side + row // cap).astype(jnp.float32)
+        which = row // cap
+        far, close = which // n, lax.rem(which, n)
+        expert = [
+            far * side + close * n + x, far * side + y * n + close, z * side + which
+        ][way]
+        e_row = expert.astype(jnp.float32)
         s_row = lax.rem(row, cap).astype(jnp.float32)
         hit0 = (ids0 == e_row).astype(jnp.float32)
         hit1 = (ids1 == e_row).astype(jnp.float32)
@@ -104,20 +134,21 @@
         ).astype(jnp.float32).astype(jnp.bfloat16)
         count = jnp.dot(hit.astype(jnp.bfloat16), before, preferred_element_type=jnp.float32)
         pick = jnp.where(count == s_row, hit, 0.0)
-        sel[q] = pick.astype(jnp.bfloat16)
-        w = pick * (hit0 * wt0 + hit1 * wt1)
-        high = w.astype(jnp.bfloat16)
-        mix[q, 0] = high
-        mix[q, 1] = (w - high.astype(jnp.float32)).astype(jnp.bfloat16)
+        sel[way, q] = pick.astype(jnp.bfloat16)
+        if way == Z:
+            w = pick * (hit0 * wt0 + hit1 * wt1)
+            high = w.astype(jnp.bfloat16)
+            mix[q, 0] = high
+            mix[q, 1] = (w - high.astype(jnp.float32)).astype(jnp.bfloat16)
 
     @step("prep0")
     def _():
         for copy in firsts[3:]:
             copy.wait()
-        met[0, 0:2, :] = ids[...].astype(jnp.float32)
-        met[0, 2:4, :] = wts[...]
-        met[0, 4:8, :] = jnp.zeros((4, tokens), jnp.float32)
-        prep(0)
+        met[Z, 0, 0:2, :] = ids[...].astype(jnp.float32)
+        met[Z, 0, 2:4, :] = wts[...]
+        met[Z, 0, 4:8, :] = jnp.zeros((4, tokens), jnp.float32)
+        prep(Z, 0)
 
     @step("raw")
     def _():
@@ -153,27 +184,53 @@
         v = (src[:, cols(c)].astype(jnp.float32) - mu[...]) * rs[...]
         tok[0, :, cols(c)] = (v * gn[:, cols(c)] + bs[:, cols(c)]).astype(jnp.bfloat16)
 
-    def select(q, c):
-        v = jnp.dot(sel[q], tok[q, :, cols(c)], preferred_element_type=jnp.float32)
+    def select(way, q, c):
+        v = jnp.dot(sel[way, q], tok[q, :, cols(c)], preferred_element_type=jnp.float32)
         snd[q, :, cols(c)] = v.astype(jnp.bfloat16)
-        xin[q, band(p), cols(c)] = snd[q, band(p), cols(c)]
-
-    def ship(q, c):
-        for o in peers:
-            remote(
-                snd.at[q, band(o), cols(c)], xin.at[q, band(p), cols(c)],
-                s_xs.at[0], s_x.at[q], {"ep": z * side + o},
-            ).start()
-
-    def disp(q, c):
-        select(q, c)
-        ship(q, c)
+
+    def ship(way, q, c):
+        if way == Z:
+            xin[q, band(p), cols(c)] = snd[q, band(p), cols(c)]
+            for o in peers:
+                remote(
+                    snd.at[q, band(o), cols(c)], xin.at[q, band(p), cols(c)],
+                    s_xs.at[0], s_x.at[1, q], {"ep": z * side + o},
+                ).start()
+            return
+        j = steps[q]
+        for a, b in [(0, 0)] + sorted(offsets, key=lambda d: -away(d)):
+            far = turn(z, a)
+            if way == X:
+                close = turn(y, b)
+                where, to = ident(far, close, x), y * n + turn(x, j)
+            else:
+                close = turn(x, b)
+                where, to = ident(far, y, close), turn(y, j) * n + x
+            got = xin.at[role[(n - a) % n], band(to), cols(c)]
+            row = band(far * n + close)
+            if a or b:
+                remote(
+                    snd.at[q, row, cols(c)], got, s_xs.at[0], s_x.at[0, role[(n - a) % n]], where
+                ).start()
+            else:
+                xin[0, band(to), cols(c)] = snd[q, row, cols(c)]
+
+    def disp(way, q, c):
+        select(way, q, c)
+        ship(way, q, c)
+
+    def ready(q):
+        count = (side - n if q == 0 else side) * cap
+        landed(xin.at[q, pl.ds(0, count), pl.ds(0, SPLIT * wide)], s_x.at[0, q])
+        landed(xin.at[q, pl.ds(0, (side - 1) * cap), pl.ds(SPLIT * wide, (k - SPLIT) * wide)], s_x.at[1, q])
 
     @step("early")
     def _():
-        for c in range(EARLY):
+        for c, _ in SIDEWAYS:
             fresh(c)
-            select(0, c)
+        for c in range(SPLIT, SPLIT + EARLY):
+            fresh(c)
+            select(Z, 0, c)
 
     @step("meet")
     def _():
@@ -181,8 +238,12 @@
 
     @step("own")
     def _():
-        for to, slot in [(up, 2), (back, 1), (over, 3)]:
-            remote(met.at[0], met.at[slot], s_met.at[0], s_met.at[1], plane(to)).start()
+        for way in (Z, X, Y):
+            for q in range(1, n):
+                slot = role[n - steps[q]]
+                remote(
+                    met.at[Z, 0], met.at[way, slot], s_met.at[3], s_met.at[way], ring(way, steps[q])
+                ).start()
 
     def others(ref, q):
         return ref.at[q, pl.ds(0, (side - 1) * cap)]
@@ -256,76 +317,86 @@
         (gw.at[0], wg.at[core]), (uw.at[0], wu.at[core]), (dw.at[0], wd.at[halfrows]),
     ]
 
+    def around(way, c):
+        send_tok(way, 0, c, up, 2)
+        send_tok(way, 0, c, back, 1)
+
     def spread(c):
-        send_tok(0, c, up, 2)
-        send_tok(0, c, back, 1)
-        ship(0, c)
+        around(Z, c)
+        ship(Z, 0, c)
 
     def first(c):
         fresh(c)
-        select(0, c)
+        select(Z, 0, c)
         spread(c)
 
     @step("disp0")
     def _():
-        pl.loop(0, EARLY)(spread)
+        for c, way in SIDEWAYS:
+            around(way, c)
+        pl.loop(SPLIT, SPLIT + EARLY)(spread)
         for i, (a, b) in enumerate(pairs):
             pltpu.make_async_copy(a, b, s_w.at[i]).start()
             remote(a, b, s_ws.at[i // 2], s_w.at[i], {"tp": 1 - core}).start()
-        pl.loop(EARLY, k)(first)
+        pl.loop(SPLIT + EARLY, k)(first)
 
     @step("preps")
     def _():
-        landed(met.at[pl.ds(1, n - 1)], s_met.at[1])
-        for q in (1, 2, 3):
-            prep(q)
-
-    @step("disp12a")
-    def _():
-        @pl.loop(0, HALF)
+        for way in (Z, X, Y):
+            landed(met.at[way, pl.ds(1, n - 1)], s_met.at[way])
+            for q in range(0 if way != Z else 1, n):
+                prep(way, q)
+
+    @step("besxy")
+    def _():
+        for c, way in SIDEWAYS:
+            arrived(c)
+            send_tok(way, 2, c, up, 3, 0)
+            send_tok(way, 1, c, back, 3, 1)
+        for c, way in SIDEWAYS:
+            for q in range(3):
+                disp(way, q, c)
+
+    @step("besza")
+    def _():
+        @pl.loop(SPLIT, MIDDLE)
         def _(c):
             arrived(c)
-            send_tok(2, c, up, 3)
-            disp(1, c)
-            disp(2, c)
-
-    @step("disp12b")
-    def _():
-        @pl.loop(HALF, k)
+            send_tok(Z, 2, c, up, 3)
+            disp(Z, 1, c)
+            disp(Z, 2, c)
+
+    @step("acrxy")
+    def _():
+        for c, way in SIDEWAYS:
+            landed(tok.at[3, :, cols(c)], s_tok.at[k + c])
+            disp(way, 3, c)
+
+    @step("beszb")
+    def _():
+        @pl.loop(MIDDLE, k)
         def _(c):
             arrived(c)
-            send_tok(1, c, back, 3)
-            disp(1, c)
-            disp(2, c)
+            send_tok(Z, 1, c, back, 3)
+            disp(Z, 1, c)
+            disp(Z, 2, c)
+
+    @step("acrz")
+    def _():
+        @pl.loop(0, MIDDLE - SPLIT)
+        def _(i):
+            arrived(k + SPLIT + i)
+            disp(Z, 3, SPLIT + i)
+            disp(Z, 3, MIDDLE + i)
 
     @step("weights")
     def _():
         for i, ref in enumerate((wg, wu, wd)):
             landed(ref, s_w.at[i])
 
-    @step("in0")
-    def _():
-        landed(others(xin, 0), s_x.at[0])
-
-    turns = 2 * per // HALF if 2 * per >= HALF else 1
-
-    @step("disp3gate0")
-    def _():
-        @pl.loop(0, HALF)
-        def _(i):
-            arrived(k + i)
-            for c in (i, i + HALF):
-                disp(3, c)
-            for j in range(turns):
-                gate(0, i * turns + j)
-
-    @step("product0")
-    def _():
-        pl.loop(0, k)(lambda c: product(0, c))
-
     @step("in1")
     def _():
-        landed(others(xin, 1), s_x.at[1])
+        ready(1)
 
     @step("gates1")
     def _():
@@ -337,7 +408,7 @@
 
     @step("in2")
     def _():
-        landed(others(xin, 2), s_x.at[2])
+        ready(2)
 
     @step("gates2")
     def _():
@@ -349,7 +420,7 @@
 
     @step("in3")
     def _():
-        landed(others(xin, 3), s_x.at[3])
+        ready(3)
 
     @step("gates3")
     def _():
@@ -365,24 +436,24 @@
             combine(1, i + HALF, up, 0, False)
             combine(2, i, back, 1, False)
 
-    @step("down12")
+    @step("down12c3")
     def _():
         @pl.loop(0, HALF)
         def _(i):
             down(1, i)
             down(2, i + HALF)
-
-    @step("give0")
-    def _():
-        pl.loop(0, k)(lambda c: give(0, c))
-
-    @step("comb3")
-    def _():
-        @pl.loop(0, HALF)
-        def _(i):
             back_in(3, i)
             combine(3, i, up, 2, False)
             combine(3, i + HALF, back, 2, False)
+
+    @step("gates0")
+    def _():
+        ready(0)
+        gates(0)
+
+    @step("down0")
+    def _():
+        pl.loop(0, k)(lambda c: down(0, c))
 
     @step("comb12b")
     def _():
@@ -395,7 +466,7 @@
 
     @step("drain")
     def _():
-        landed(met.at[pl.ds(1, n - 1)], s_met.at[0])
+        landed(met.at[:, pl.ds(1, n - 1)], s_met.at[3])
         landed(wg, s_ws.at[0])
         landed(wd.at[halfrows], s_ws.at[1])
         landed(tok.at[pl.ds(0, n - 1)], s_toks.at[0])
@@ -448,11 +519,11 @@
             pltpu.VMEM((2, count), jnp.int32),
             pltpu.VMEM((2, count), jnp.float32),
             pltpu.VMEM((LINE, count, width), bf),
-            pltpu.VMEM((LINE, 8, count), jnp.float32),
+            pltpu.VMEM((3, LINE, 8, count), jnp.float32),
             pltpu.VMEM((2, width, half), bf),
             pltpu.VMEM((2, width, half), bf),
             pltpu.VMEM((2 * half, width), bf),
-            pltpu.VMEM((LINE, rows, count), bf),
+            pltpu.VMEM((3, LINE, rows, count), bf),
             pltpu.VMEM((LINE, 2, rows, count), bf),
             pltpu.VMEM((LINE, rows, width), bf),
             pltpu.VMEM((LINE, rows, width), bf),
@@ -462,12 +533,12 @@
             pltpu.VMEM((LINE - 1, CHUNKS, count, wide), bf),
             pltpu.VMEM((LINE - 1, CHUNKS, count, wide), bf),
             dma((5,)),
-            dma((2,)),
+            dma((4,)),
             dma((3,)),
             dma((2,)),
-            dma((CHUNKS + HALF,)),
+            dma((CHUNKS + MIDDLE,)),
             dma((1,)),
-            dma((LINE,)),
+            dma((2, LINE)),
             dma((1,)),
             dma((2 * CHUNKS + HALF,)),
             dma((1,)),

time: 101 us -> 101 us (level)
  no operation moved by 1% of the time
where the time goes in v5:
time: 101 us
  Pallas kernels  99.5 us (99%)
    pallas_call x1, Pallas kernels, body(): pl.pallas_call(functools.partial(kernel, side), out_shape=pltpu.VMEM((cou...  99.5 us

profile of v5, /device:TPU:0, one launch (start us, length us, event | category | flops | bytes accessed | tf_op | source)
XLA Modules:
  0.0 100.5 jit_solution(12500674165370595457)
XLA Ops:
  0.0 99.5 %shard_map.82 = bf16[256,2048]{1,0:T(8,128)(2,1)S(1)} custom-call(bf16[256,2048]{1,0:T(8,128)(2,1)} %raw.1, f32[1,2048]{1,0:T(1,128)} %bitcast.4, f32[1,2048]{1,0:T(1,128)} %bitcast.5, s32[2,256]{1,0:T(2,128)} %bitcast.6, f32[2,256]{1,0:T(2,128)} %bitcast.7, bf16[1,2048,512]{2,1,0:T(8,128)(2,1)} %gw.1, bf16[1,2048,512]{2,1,0:T(8,128)(2,1)} %uw.1, ...), custom_call_target="tpu_custom_call" | custom-call | tf_op jit(solution)/shard_map/pallas_call | solution.py:507
  99.6 1.0 copy.10

commit v6 on v5

--- a/solution.py
+++ b/solution.py
@@ -11,7 +11,7 @@
 LINE = 4
 CHUNKS = 8
 HALF = CHUNKS // 2
-EARLY = 2
+EARLY = 1
 X, Y, Z = 0, 1, 2
 SIDEWAYS = [(0, X), (1, Y)]
 SPLIT = len(SIDEWAYS)
@@ -226,8 +226,6 @@
 
     @step("early")
     def _():
-        for c, _ in SIDEWAYS:
-            fresh(c)
         for c in range(SPLIT, SPLIT + EARLY):
             fresh(c)
             select(Z, 0, c)
@@ -332,9 +330,10 @@
 
     @step("disp0")
     def _():
+        pl.loop(SPLIT, SPLIT + EARLY)(spread)
         for c, way in SIDEWAYS:
+            fresh(c)
             around(way, c)
-        pl.loop(SPLIT, SPLIT + EARLY)(spread)
         for i, (a, b) in enumerate(pairs):
             pltpu.make_async_copy(a, b, s_w.at[i]).start()
             remote(a, b, s_ws.at[i // 2], s_w.at[i], {"tp": 1 - core}).start()

time: 101 us -> 101 us (level)
  no operation moved by 1% of the time
where the time goes in v6:
time: 101 us; the launch traced here: 100 us
  Pallas kernels  99.4 us (98%)
    pallas_call x1, Pallas kernels, body(): pl.pallas_call(functools.partial(kernel, side), out_shape=pltpu.VMEM((cou...  99.4 us

profile of v6, /device:TPU:0, one launch (start us, length us, event | category | flops | bytes accessed | tf_op | source)
XLA Modules:
  0.0 100.4 jit_solution(124785877264254837)
XLA Ops:
  0.0 99.4 %shard_map.82 = bf16[256,2048]{1,0:T(8,128)(2,1)S(1)} custom-call(bf16[256,2048]{1,0:T(8,128)(2,1)} %raw.1, f32[1,2048]{1,0:T(1,128)} %bitcast.4, f32[1,2048]{1,0:T(1,128)} %bitcast.5, s32[2,256]{1,0:T(2,128)} %bitcast.6, f32[2,256]{1,0:T(2,128)} %bitcast.7, bf16[1,2048,512]{2,1,0:T(8,128)(2,1)} %gw.1, bf16[1,2048,512]{2,1,0:T(8,128)(2,1)} %uw.1, ...), custom_call_target="tpu_custom_call" | custom-call | tf_op jit(solution)/shard_map/pallas_call | solution.py:506
  99.4 1.0 copy.10

commit v7 on v6

--- a/solution.py
+++ b/solution.py
@@ -155,7 +155,7 @@
         for copy in firsts[:3]:
             copy.wait()
 
-    slab = min(32, tokens)
+    slab = min(16, tokens)
     lanes = part.shape[1]
 
     @step("stats")

time: 101 us -> 101 us (level)
  no operation moved by 1% of the time
where the time goes in v7:
time: 101 us
  Pallas kernels  99.9 us (99%)
    pallas_call x1, Pallas kernels, body(): pl.pallas_call(functools.partial(kernel, side), out_shape=pltpu.VMEM((cou...  99.9 us

profile of v7, /device:TPU:0, one launch (start us, length us, event | category | flops | bytes accessed | tf_op | source)
XLA Modules:
  0.0 100.9 jit_solution(17293260652010511026)
XLA Ops:
  0.0 99.9 %shard_map.82 = bf16[256,2048]{1,0:T(8,128)(2,1)S(1)} custom-call(bf16[256,2048]{1,0:T(8,128)(2,1)} %raw.1, f32[1,2048]{1,0:T(1,128)} %bitcast.4, f32[1,2048]{1,0:T(1,128)} %bitcast.5, s32[2,256]{1,0:T(2,128)} %bitcast.6, f32[2,256]{1,0:T(2,128)} %bitcast.7, bf16[1,2048,512]{2,1,0:T(8,128)(2,1)} %gw.1, bf16[1,2048,512]{2,1,0:T(8,128)(2,1)} %uw.1, ...), custom_call_target="tpu_custom_call" | custom-call | tf_op jit(solution)/shard_map/pallas_call | solution.py:506
  99.9 1.0 copy.10
